TPU v7x, 32 devices: a whole 2x2x4 slice. The times are simulated.
32 devices in a mesh: sp: 8 (over z, y), tp: 4 (over x, core).
Axes of the slice: x: 2, y: 2, z: 4, core: 2. Of those that a mesh axis runs over, the one named last changes fastest.
Arguments:
- inputs: bfloat16 [4096, 4096], P('sp', 'tp'), may hold values from -24 to 24
- length: int32 [1], replicated, may hold values from 2049 to 4096
- win_query: bfloat16 [4096, 1536], P(None, 'tp'), may hold values from -8 to 8
- win_key: bfloat16 [4096, 512], P(None, 'tp'), may hold values from -8 to 8
- win_value: bfloat16 [4096, 512], P(None, 'tp'), may hold values from -1.5 to 1.5
- sink_logit: float32 [24], P('tp'), may hold values from 4 to 8
- diff_query: bfloat16 [4096, 1024], P(None, 'tp'), may hold values from -8 to 8
- diff_key: bfloat16 [4096, 1024], P(None, 'tp'), may hold values from -8 to 8
- diff_value: bfloat16 [4096, 1024], P(None, 'tp'), may hold values from -0.09375 to 0.09375
- mix_lambda: float32 [16], P('tp'), may hold values from 0.3 to 0.8
- head_gain: float32 [64], replicated, may hold values from 0.1 to 1.9
- win_out: bfloat16 [1536, 4096], P('tp'), may hold values from -0.125 to 0.125
- diff_out: bfloat16 [1024, 4096], P('tp'), may hold values from -0.125 to 0.125
Outputs:
- merged_out: bfloat16 [4096, 4096], P(('sp', 'tp'))
All inputs are finite; a program needn't handle non-finite values.
Results may differ from a plain program's by a relative error of at most 0.015.
Values may be sent and summed in bfloat16 or wider, within the bound.
No kernel may reach another device: no remote copies, remote signals or barrier semaphores. Data moves between devices by JAX's collectives and lax.ppermute only.
A program may use at most 128 MiB of HBM per device.

v0:
```python
import jax
import jax.numpy as jnp
from jax import lax
from jax.sharding import PartitionSpec as P

HEAD = 64
DQK = 32
GROUP = 3
WINDOW = 128
epsilon = 1e-06
masked_score = -1e30


def extended(block, sides, width):
    for axis, dim in sides:
        count = lax.axis_size(axis)
        forward = [(i, i + 1) for i in range(count - 1)]
        backward = [(target, source) for source, target in forward]
        low = lax.ppermute(
            lax.slice_in_dim(block, block.shape[dim] - width, None, axis=dim), axis, forward
        )
        high = lax.ppermute(lax.slice_in_dim(block, 0, width, axis=dim), axis, backward)
        block = jnp.concatenate([low, block, high], axis=dim)
    return block


def window_part(win_q, win_k, win_v, sink_logit, live_count, offset):
    row_count = win_q.shape[0]
    kv_local = win_k.shape[1] // HEAD
    stacked = jnp.stack(
        (win_k.reshape(row_count, kv_local, HEAD), win_v.reshape(row_count, kv_local, HEAD)), axis=2
    )
    stacked = stacked.reshape(row_count, kv_local * 2 * HEAD)
    padded = extended(stacked, (("sp", 0),), WINDOW)
    padded = padded.reshape(row_count + 2 * WINDOW, kv_local, 2, HEAD)
    keys_win = padded[:, :, 0]
    values_win = padded[:, :, 1]
    queries = win_q.reshape(row_count, kv_local, GROUP, HEAD)
    sink_table = sink_logit.reshape(kv_local, GROUP)
    query_pos = offset + jnp.arange(row_count, dtype=jnp.int32)
    key_pos = offset - WINDOW + jnp.arange(row_count + 2 * WINDOW, dtype=jnp.int32)
    allowed = (
        (jnp.abs(query_pos[:, None] - key_pos[None, :]) <= WINDOW)
        & (key_pos[None, :] >= 0)
        & (key_pos[None, :] < live_count)
    )
    scores = jnp.einsum(
        "qhgd,khd->hgqk", queries, keys_win, preferred_element_type=jnp.float32
    ) * HEAD ** (-0.5)
    scores = jnp.where(allowed[None, None], scores, masked_score)
    row_max = jnp.maximum(jnp.max(scores, axis=-1), sink_table[:, :, None])
    exponent = jnp.where(allowed[None, None], jnp.exp(scores - row_max[..., None]), 0.0)
    denominator = jnp.sum(exponent, axis=-1) + jnp.exp(sink_table[:, :, None] - row_max)
    result = jnp.einsum(
        "hgqk,khd->qhgd",
        exponent.astype(jnp.bfloat16),
        values_win,
        preferred_element_type=jnp.float32,
    )
    result = result / jnp.transpose(denominator, (2, 0, 1))[..., None]
    result = jnp.where((query_pos < live_count)[:, None, None, None], result, 0.0)
    return result.reshape(row_count, kv_local * GROUP * HEAD).astype(jnp.bfloat16)


def attend(running, queries, key_part, value_part, live_count, block_total, query_step):
    key_length = key_part.shape[0]
    key_step = 4096

    def one_query_block(block_index, block_state):
        running_max, total_sum, weighted = block_state
        row_begin = block_index * query_step
        query_slab = lax.dynamic_slice_in_dim(queries, row_begin, query_step, 0)
        start_state = (
            lax.dynamic_slice_in_dim(running_max, row_begin, query_step, 2),
            lax.dynamic_slice_in_dim(total_sum, row_begin, query_step, 2),
            lax.dynamic_slice_in_dim(weighted, row_begin, query_step, 2),
        )

        def one_key_block(key_index, key_state):
            block_max, block_sum, block_weighted = key_state
            key_begin = key_index * key_step
            key_slab = lax.dynamic_slice_in_dim(key_part, key_begin, key_step, 0)
            value_slab = lax.dynamic_slice_in_dim(value_part, key_begin, key_step, 0)
            key_pos = key_begin + jnp.arange(key_step, dtype=jnp.int32)
            allowed = key_pos < live_count
            scores = jnp.einsum(
                "qhmd,khmd->hmqk", query_slab, key_slab, preferred_element_type=jnp.float32
            ) * DQK ** (-0.5)
            scores = jnp.where(allowed, scores, masked_score)
            new_max = jnp.maximum(block_max, jnp.max(scores, axis=-1))
            rescale = jnp.exp(block_max - new_max)
            exponent = jnp.where(allowed, jnp.exp(scores - new_max[..., None]), 0.0)
            new_total = block_sum * rescale + jnp.sum(exponent, axis=-1)
            new_weighted = block_weighted * rescale[..., None] + jnp.einsum(
                "hmqk,khd->hmqd",
                exponent.astype(jnp.bfloat16),
                value_slab,
                preferred_element_type=jnp.float32,
            )
            return (new_max, new_total, new_weighted)

        final_state = lax.fori_loop(0, key_length // key_step, one_key_block, start_state)
        return (
            lax.dynamic_update_slice_in_dim(running_max, final_state[0], row_begin, 2),
            lax.dynamic_update_slice_in_dim(total_sum, final_state[1], row_begin, 2),
            lax.dynamic_update_slice_in_dim(weighted, final_state[2], row_begin, 2),
        )

    return lax.fori_loop(0, block_total, one_query_block, running)


def diff_part(diff_q, diff_k, diff_v, mix_lambda, head_gain, live_count, offset):
    row_count = diff_q.shape[0]
    heads_local = mix_lambda.shape[0]
    query_step = 128
    positions = offset + jnp.arange(row_count, dtype=jnp.int32)
    live_rows = jnp.sum((positions < live_count).astype(jnp.int32))
    block_total = (live_rows + query_step - 1) // query_step
    queries = diff_q.reshape(row_count, heads_local, 2, DQK)
    zero_state = (
        jnp.full((heads_local, 2, row_count), masked_score, jnp.float32),
        jnp.zeros((heads_local, 2, row_count), jnp.float32),
        jnp.zeros((heads_local, 2, row_count, HEAD), jnp.float32),
    )
    key_part = lax.all_gather(diff_k, "sp", axis=0, tiled=True).reshape(-1, heads_local, 2, DQK)
    value_part = lax.all_gather(diff_v, "sp", axis=0, tiled=True).reshape(-1, heads_local, HEAD)
    running = lax.cond(
        jnp.int32(0) < live_count,
        lambda inner_state: attend(
            inner_state, queries, key_part, value_part, live_count, block_total, query_step
        ),
        lambda inner_state: inner_state,
        zero_state,
    )
    total_sum = running[1]
    safe_total = jnp.where(total_sum > 0.0, total_sum, 1.0)
    map_rows = running[2] / safe_total[..., None]
    mixed_rows = map_rows[:, 0] - mix_lambda[:, None, None] * map_rows[:, 1]
    normed = (
        mixed_rows
        * lax.rsqrt(jnp.mean(mixed_rows * mixed_rows, axis=-1, keepdims=True) + epsilon)
        * head_gain
    )
    normed = jnp.where((positions < live_count)[None, :, None], normed, 0.0)
    result = (
        jnp.transpose(normed, (1, 0, 2)).reshape(row_count, heads_local * HEAD).astype(jnp.bfloat16)
    )
    return result


def body(
    inputs,
    length,
    win_query,
    win_key,
    win_value,
    sink_logit,
    diff_query,
    diff_key,
    diff_value,
    mix_lambda,
    head_gain,
    win_out,
    diff_out,
):
    row_count = inputs.shape[0]
    live_count = length[0]
    weights = (win_query, win_key, win_value, diff_query, diff_key, diff_value)
    segment = lax.all_gather(inputs, "tp", axis=1, tiled=True)
    summed = tuple(
        (jnp.dot(segment, weight, preferred_element_type=jnp.float32) for weight in weights)
    )
    win_q, win_k, win_v, diff_q, diff_k, diff_v = [total.astype(jnp.bfloat16) for total in summed]
    offset = lax.axis_index("sp") * row_count
    win_rows = window_part(win_q, win_k, win_v, sink_logit, live_count, offset)
    diff_rows = diff_part(diff_q, diff_k, diff_v, mix_lambda, head_gain, live_count, offset)
    partial_value = jnp.dot(win_rows, win_out, preferred_element_type=jnp.float32)
    return lax.psum_scatter(
        (partial_value + jnp.dot(diff_rows, diff_out, preferred_element_type=jnp.float32)).astype(
            jnp.bfloat16
        ),
        "tp",
        scatter_dimension=0,
        tiled=True,
    )


def solution(mesh):
    placed = (
        P("sp", "tp"),
        P(),
        P(None, "tp"),
        P(None, "tp"),
        P(None, "tp"),
        P("tp"),
        P(None, "tp"),
        P(None, "tp"),
        P(None, "tp"),
        P("tp"),
        P(),
        P("tp", None),
        P("tp", None),
    )
    return jax.shard_map(
        body, mesh=mesh, in_specs=placed, out_specs=P(("sp", "tp"), None), check_vma=False
    )
```

profile of v0, /device:TPU:0, one launch (start us, length us, event | category | flops | bytes accessed | tf_op | source)
XLA Modules:
  0.0 299.4 jit_solution(1611999572940378291)
XLA Ops:
  7.3 38.8 %all-gather.4.cloned.1.call-done = bf16[512,4096]{1,0:T(8,128)(2,1)} async-done(((bf16[512,1024]{1,0:T(8,128)(2,1)}), bf16[512,4096]{1,0:T(8,128)(2,1)}) %all-gather.4.cloned.1.call-update) | async-done | bytes 4194320 | tf_op jit(solution)/shard_map/all_gather | solution.py:169
  46.1 4.8 %convolution_convert_fusion.1 = bf16[512,256]{1,0:T(8,128)(2,1)} fusion(bf16[512,4096]{1,0:T(8,128)(2,1)} %all-gather.4.cloned.1.call-done, bf16[4096,256]{1,0:T(8,128)(2,1)} %param.25), kind=kOutput, calls=%fused_computation.34 | convolution fusion | flops 1073872896 | bytes 6553600 | tf_op jit(solution)/shard_map/dot_general | solution.py:171
  52.6 4.4 %convolution_convert_fusion.4 = bf16[512,128]{0,1:T(8,128)(2,1)S(1)} fusion(bf16[512,4096]{1,0:T(8,128)(2,1)} %all-gather.4.cloned.1.call-done, bf16[4096,128]{1,0:T(8,128)(2,1)} %param.21), kind=kOutput, calls=%fused_computation.37 | convolution fusion | flops 536936448 | bytes 5373952 | tf_op jit(solution)/shard_map/dot_general | solution.py:171
  61.8 5.2 %collective-permute-start = (bf16[128,256]{0,1:T(8,128)(2,1)}, bf16[128,256]{0,1:T(8,128)(2,1)}, u32[]{:S(2)}, u32[]{:S(2)}) collective-permute-start(bf16[128,256]{0,1:T(8,128)(2,1)} %bitcast.8), channel_id=1, source_target_pairs={{0,4},{4,8},{8,12},{12,16},{16,20},{20,24},{24,28},{1,5},{5,9},{9,... | collective-permute-start | bytes 196616 | tf_op jit(solution)/shard_map/ppermute | solution.py:19
  69.2 5.2 %convolution_convert_fusion = bf16[512,384]{0,1:T(8,128)(2,1)S(1)} fusion(bf16[512,4096]{1,0:T(8,128)(2,1)} %all-gather.4.cloned.1.call-done, bf16[4096,384]{1,0:T(8,128)(2,1)} %param.19), kind=kOutput, calls=%fused_computation.33 | convolution fusion | flops 1610809344 | bytes 7733248 | tf_op jit(solution)/shard_map/dot_general | solution.py:171
  84.1 5.6 %fusion.52 = f32[512,4096]{1,0:T(8,128)} fusion(bf16[512,384]{0,1:T(8,128)(2,1)S(1)} %bitcast.123, bf16[384,4096]{1,0:T(8,128)(2,1)S(1)} %copy-done), kind=kOutput, calls=%fused_computation.68 | convolution fusion | flops 1610612736 | bytes 11927552 | tf_op jit(solution)/shard_map/dot_general | solution.py:177
  89.7 11.3 %all-gather.8.cloned.1.call-done = bf16[4096,256]{1,0:T(8,128)(2,1)} async-done(((bf16[512,256]{1,0:T(8,128)(2,1)}), bf16[4096,256]{1,0:T(8,128)(2,1)}) %all-gather.8.cloned.1.call-update) | async-done | bytes 2097168 | tf_op jit(solution)/shard_map/all_gather | solution.py:126
  101.0 49.8 %all-gather.6.cloned.1.call-done = bf16[4096,256]{1,0:T(8,128)(2,1)} async-done(((bf16[512,256]{1,0:T(8,128)(2,1)}), bf16[4096,256]{1,0:T(8,128)(2,1)}) %all-gather.6.cloned.1.call-update) | async-done | bytes 2097168 | tf_op jit(solution)/shard_map/all_gather | solution.py:125
  150.8 89.2 %conditional.1 = (f32[4,2,512]{2,1,0:T(2,128)}, f32[4,2,512,64]{2,3,1,0:T(8,128)}) conditional(s32[]{:T(128)} %convert_element_type.55, () %tuple.34, (s32[512]{0:T(512)S(1)}, bf16[512,256]{1,0:T(8,128)(2,1)S(1)}, bf16[4096,256]{1,0:T(8,128)(2,1)}, bf16[4096,256]{1,0:T(8,128)(2,1)}, s32[]{:T(128)}, /*index=5*/s32[]{:T(128)}) %tuple.79), branch_computations={%region_3.4_spmd, %region_4.9_spmd.clone} | conditional | flops 859970048 | bytes 132364824 | solution.py:127
  152.3 4.1 %copy.34 = bf16[4096,256]{0,1:T(8,128)(2,1)} copy(bf16[4096,256]{1,0:T(8,128)(2,1)} %get-tuple-element.250) | data formatting | bytes 4194304 | tf_op jit(solution)/shard_map
  156.4 2.9 copy.33
  161.0 79.0 %while.37 = (s32[]{:T(128)}, f32[4,2,512]{2,1,0:T(2,128)S(1)}, f32[4,2,512]{2,1,0:T(2,128)}, f32[4,2,512,64]{2,3,1,0:T(8,128)}, s32[]{:T(128)}, /*index=5*/s32[]...) while((s32[]{:T(128)}, f32[4,2,512]{2,1,0:T(2,128)S(1)}, ...), condition=%wide.region_8.8_spmd, body=%wide.region_5.7_spmd.sunk | while | flops 859969536 | bytes 122368224 | solution.py:109
  164.5 4.9 %fusion.83 = f32[4,2,128]{2,1,0:T(2,128)S(1)} fusion(f32[4,2,128,4096]{3,2,1,0:T(8,128)S(1)} %get-tuple-element.357, f32[4,2,128]{2,1,0:T(2,128)S(1)} %get-tuple-element.358, pred[4096]{0:T(1024)(128)(4,1)S(1)} %iota_compare_fusion.2), kind=kLoop, calls=%fused_computation.4.clone.1 | loop fusion | flops 20970496 | bytes 16789504 | tf_op jit(solution)/shard_map/cond/branch_1_fun/while/body/while/body/eval_jaxpr/reduce_sum | solution.py:93
  171.5 9.3 %fusion.84 = f32[4,2,512,64]{2,3,1,0:T(8,128)} fusion(f32[4,2,512,64]{2,3,1,0:T(8,128)} %get-tuple-element.377, s32[]{:T(128)S(6)} %select_n.128, bf16[4096,4,64]{0,2,1:T(8,128)(2,1)} %get-tuple-element.395, f32[4,2,128,4096]{3,2,1,0:T(8,128)} %copy-done.2, f32[4,2,128]{2,1,0:T(2,128)S(1)} %get-tuple-element.358, ...), kind=kOutput, calls=%fused_computation.9.clone.1 | convolution fusion | flops 557973504 | bytes 19410948 | tf_op jit(solution)/shard_map/cond/branch_1_fun/while/body/while/body/eval_jaxpr/hmqk,khd->hmqd/dot_general | solution.py:94
  184.2 4.9 %fusion.83 = f32[4,2,128]{2,1,0:T(2,128)S(1)} fusion(f32[4,2,128,4096]{3,2,1,0:T(8,128)S(1)} %get-tuple-element.357, f32[4,2,128]{2,1,0:T(2,128)S(1)} %get-tuple-element.358, pred[4096]{0:T(1024)(128)(4,1)S(1)} %iota_compare_fusion.2), kind=kLoop, calls=%fused_computation.4.clone.1 | loop fusion | flops 20970496 | bytes 16789504 | tf_op jit(solution)/shard_map/cond/branch_1_fun/while/body/while/body/eval_jaxpr/reduce_sum | solution.py:93
  191.2 9.3 %fusion.84 = f32[4,2,512,64]{2,3,1,0:T(8,128)} fusion(f32[4,2,512,64]{2,3,1,0:T(8,128)} %get-tuple-element.377, s32[]{:T(128)S(6)} %select_n.128, bf16[4096,4,64]{0,2,1:T(8,128)(2,1)} %get-tuple-element.395, f32[4,2,128,4096]{3,2,1,0:T(8,128)} %copy-done.2, f32[4,2,128]{2,1,0:T(2,128)S(1)} %get-tuple-element.358, ...), kind=kOutput, calls=%fused_computation.9.clone.1 | convolution fusion | flops 557973504 | bytes 19410948 | tf_op jit(solution)/shard_map/cond/branch_1_fun/while/body/while/body/eval_jaxpr/hmqk,khd->hmqd/dot_general | solution.py:94
  201.2 2.7 fusion.82
  204.0 4.9 %fusion.83 = f32[4,2,128]{2,1,0:T(2,128)S(1)} fusion(f32[4,2,128,4096]{3,2,1,0:T(8,128)S(1)} %get-tuple-element.357, f32[4,2,128]{2,1,0:T(2,128)S(1)} %get-tuple-element.358, pred[4096]{0:T(1024)(128)(4,1)S(1)} %iota_compare_fusion.2), kind=kLoop, calls=%fused_computation.4.clone.1 | loop fusion | flops 20970496 | bytes 16789504 | tf_op jit(solution)/shard_map/cond/branch_1_fun/while/body/while/body/eval_jaxpr/reduce_sum | solution.py:93
  211.0 9.3 %fusion.84 = f32[4,2,512,64]{2,3,1,0:T(8,128)} fusion(f32[4,2,512,64]{2,3,1,0:T(8,128)} %get-tuple-element.377, s32[]{:T(128)S(6)} %select_n.128, bf16[4096,4,64]{0,2,1:T(8,128)(2,1)} %get-tuple-element.395, f32[4,2,128,4096]{3,2,1,0:T(8,128)} %copy-done.2, f32[4,2,128]{2,1,0:T(2,128)S(1)} %get-tuple-element.358, ...), kind=kOutput, calls=%fused_computation.9.clone.1 | convolution fusion | flops 557973504 | bytes 19410948 | tf_op jit(solution)/shard_map/cond/branch_1_fun/while/body/while/body/eval_jaxpr/hmqk,khd->hmqd/dot_general | solution.py:94
  221.0 2.7 fusion.82
  223.7 4.9 %fusion.83 = f32[4,2,128]{2,1,0:T(2,128)S(1)} fusion(f32[4,2,128,4096]{3,2,1,0:T(8,128)S(1)} %get-tuple-element.357, f32[4,2,128]{2,1,0:T(2,128)S(1)} %get-tuple-element.358, pred[4096]{0:T(1024)(128)(4,1)S(1)} %iota_compare_fusion.2), kind=kLoop, calls=%fused_computation.4.clone.1 | loop fusion | flops 20970496 | bytes 16789504 | tf_op jit(solution)/shard_map/cond/branch_1_fun/while/body/while/body/eval_jaxpr/reduce_sum | solution.py:93
  230.7 9.3 %fusion.84 = f32[4,2,512,64]{2,3,1,0:T(8,128)} fusion(f32[4,2,512,64]{2,3,1,0:T(8,128)} %get-tuple-element.377, s32[]{:T(128)S(6)} %select_n.128, bf16[4096,4,64]{0,2,1:T(8,128)(2,1)} %get-tuple-element.395, f32[4,2,128,4096]{3,2,1,0:T(8,128)} %copy-done.2, f32[4,2,128]{2,1,0:T(2,128)S(1)} %get-tuple-element.358, ...), kind=kOutput, calls=%fused_computation.9.clone.1 | convolution fusion | flops 557973504 | bytes 19410948 | tf_op jit(solution)/shard_map/cond/branch_1_fun/while/body/while/body/eval_jaxpr/hmqk,khd->hmqd/dot_general | solution.py:94
  242.7 6.8 %add_convert_fusion = bf16[512,4096]{1,0:T(8,128)(2,1)} fusion(f32[512,4096]{1,0:T(8,128)} %fusion.52, bf16[512,256]{0,1:T(8,128)(2,1)S(1)} %bitcast.122, bf16[256,4096]{1,0:T(8,128)(2,1)S(1)} %copy-done.5), kind=kOutput, calls=%fused_computation.23 | convolution fusion | flops 1077936128 | bytes 14942208 | tf_op jit(solution)/shard_map/dot_general | solution.py:179
  249.6 43.2 %reduce-scatter.2.cloned.1.call-done = bf16[128,4096]{1,0:T(8,128)(2,1)} async-done(((bf16[512,4096]{1,0:T(8,128)(2,1)}), bf16[128,4096]{1,0:T(8,128)(2,1)}) %reduce-scatter.2.cloned.1.call-update) | async-done | bytes 1048592 | tf_op jit(solution)/shard_map/reduce_scatter | solution.py:178
  (101 shorter events, 40.1 us)
Async XLA Ops:
  6.5 77.6 %copy-start = (bf16[384,4096]{1,0:T(8,128)(2,1)S(1)}, bf16[384,4096]{1,0:T(8,128)(2,1)}, u32[]{:S(2)}) copy-start(bf16[384,4096]{1,0:T(8,128)(2,1)} %param.28) | copy-start | bytes 9437188
  6.5 39.6 %all-gather.4.cloned.1.call-start = ((), (), s32[]{:S(2)}) async-start(), calls=%async_computation.1 | async-start | bytes 5242880 | tf_op jit(solution)/shard_map/all_gather | solution.py:169
  7.3 44.4 %copy-start.16 = (f32[6]{0:T(128)S(1)}, f32[6]{0:T(128)}, u32[]{:S(2)}) copy-start(f32[6]{0:T(128)} %param.22) | copy-start | bytes 76
  7.3 93.7 %all-gather.8.cloned.1.call-start = ((), (), s32[]{:S(2)}) async-start(), calls=%async_computation.3 | async-start | bytes 2359296 | tf_op jit(solution)/shard_map/all_gather | solution.py:126
  51.0 99.8 %all-gather.6.cloned.1.call-start = ((), (), s32[]{:S(2)}) async-start(), calls=%async_computation.2 | async-start | bytes 2359296 | tf_op jit(solution)/shard_map/all_gather | solution.py:125
  51.8 5.2 %copy-start.3 = (bf16[512,4096]{1,0:T(8,128)(2,1)S(1)}, bf16[512,4096]{1,0:T(8,128)(2,1)}, u32[]{:S(2)}) copy-start(bf16[512,4096]{1,0:T(8,128)(2,1)} %all-gather.4.cloned.1.call-done) | copy-start | bytes 12582916
  51.8 5.2 %copy-start.10 = (bf16[4096,128]{1,0:T(8,128)(2,1)S(1)}, bf16[4096,128]{1,0:T(8,128)(2,1)}, u32[]{:S(2)}) copy-start(bf16[4096,128]{1,0:T(8,128)(2,1)} %param.20) | copy-start | bytes 3145732
  57.0 9.9 %copy-start.14 = (bf16[4096,256]{1,0:T(8,128)(2,1)S(1)}, bf16[4096,256]{1,0:T(8,128)(2,1)}, u32[]{:S(2)}) copy-start(bf16[4096,256]{1,0:T(8,128)(2,1)} %param.24) | copy-start | bytes 6291460
  60.5 15.9 %collective-permute-start.1 = (bf16[128,256]{0,1:T(8,128)(2,1)}, bf16[128,256]{0,1:T(8,128)(2,1)}, u32[]{:S(2)}, u32[]{:S(2)}) collective-permute-start(bf16[128,256]{0,1:T(8,128)(2,1)} %bitcast.10), channel_id=1, source_target_pairs={{4,0},{8,4},{12,8},{16,12},{20,16},{24,20},{28,24},{5,1},{9,5},{13... | collective-permute-start | bytes 196616 | tf_op jit(solution)/shard_map/ppermute | solution.py:22
  61.8 14.6 %collective-permute-start = (bf16[128,256]{0,1:T(8,128)(2,1)}, bf16[128,256]{0,1:T(8,128)(2,1)}, u32[]{:S(2)}, u32[]{:S(2)}) collective-permute-start(bf16[128,256]{0,1:T(8,128)(2,1)} %bitcast.8), channel_id=1, source_target_pairs={{0,4},{4,8},{8,12},{12,16},{16,20},{20,24},{24,28},{1,5},{5,9},{9,... | collective-permute-start | bytes 196616 | tf_op jit(solution)/shard_map/ppermute | solution.py:19
  69.0 223.9 %reduce-scatter.2.cloned.1.call-start = ((), (), s32[]{:S(2)}) async-start(), calls=%async_computation.4 | async-start | bytes 5242880 | tf_op jit(solution)/shard_map/reduce_scatter | solution.py:178
  69.2 5.2 %copy-start.4 = (bf16[512,4096]{1,0:T(8,128)(2,1)S(1)}, bf16[512,4096]{1,0:T(8,128)(2,1)}, u32[]{:S(2)}) copy-start(bf16[512,4096]{1,0:T(8,128)(2,1)} %all-gather.4.cloned.1.call-done) | copy-start | bytes 12582916
  69.2 5.2 %copy-start.15 = (bf16[4096,256]{1,0:T(8,128)(2,1)S(1)}, bf16[4096,256]{1,0:T(8,128)(2,1)}, u32[]{:S(2)}) copy-start(bf16[4096,256]{1,0:T(8,128)(2,1)} %param.23) | copy-start | bytes 6291460
  74.4 2.0 copy-start.7
  74.4 2.0 copy-start.9
  84.1 66.7 %copy-start.11 = (bf16[512,256]{1,0:T(8,128)(2,1)S(1)}, bf16[512,256]{1,0:T(8,128)(2,1)}, u32[]{:S(2)}) copy-start(bf16[512,256]{1,0:T(8,128)(2,1)} %convolution_convert_fusion.3) | copy-start | bytes 786436
  150.8 91.5 %copy-start.12 = (f32[4]{0:T(128)S(1)}, f32[4]{0:T(128)}, u32[]{:S(2)}) copy-start(f32[4]{0:T(128)} %param.26) | copy-start | bytes 52
  150.8 91.7 %copy-start.13 = (f32[64]{0:T(128)S(1)}, f32[64]{0:T(128)}, u32[]{:S(2)}) copy-start(f32[64]{0:T(128)} %param.27) | copy-start | bytes 772
  164.4 5.7 %copy-start.2 = (f32[4,2,128,4096]{3,2,1,0:T(8,128)}, f32[4,2,128,4096]{3,2,1,0:T(8,128)S(1)}, u32[]{:S(2)}) copy-start(f32[4,2,128,4096]{3,2,1,0:T(8,128)S(1)} %get-tuple-element.357) | copy-start | bytes 50331652 | tf_op jit(solution)/shard_map/cond/branch_1_fun/while
  184.2 5.7 %copy-start.2 = (f32[4,2,128,4096]{3,2,1,0:T(8,128)}, f32[4,2,128,4096]{3,2,1,0:T(8,128)S(1)}, u32[]{:S(2)}) copy-start(f32[4,2,128,4096]{3,2,1,0:T(8,128)S(1)} %get-tuple-element.357) | copy-start | bytes 50331652 | tf_op jit(solution)/shard_map/cond/branch_1_fun/while
  204.0 5.7 %copy-start.2 = (f32[4,2,128,4096]{3,2,1,0:T(8,128)}, f32[4,2,128,4096]{3,2,1,0:T(8,128)S(1)}, u32[]{:S(2)}) copy-start(f32[4,2,128,4096]{3,2,1,0:T(8,128)S(1)} %get-tuple-element.357) | copy-start | bytes 50331652 | tf_op jit(solution)/shard_map/cond/branch_1_fun/while
  223.7 5.7 %copy-start.2 = (f32[4,2,128,4096]{3,2,1,0:T(8,128)}, f32[4,2,128,4096]{3,2,1,0:T(8,128)S(1)}, u32[]{:S(2)}) copy-start(f32[4,2,128,4096]{3,2,1,0:T(8,128)S(1)} %get-tuple-element.357) | copy-start | bytes 50331652 | tf_op jit(solution)/shard_map/cond/branch_1_fun/while
  240.1 2.7 copy-start.5
  242.7 50.1 %copy-start.1 = (bf16[384,4096]{1,0:T(8,128)(2,1)S(1)}, bf16[384,4096]{1,0:T(8,128)(2,1)}, u32[]{:S(2)}) copy-start(bf16[384,4096]{1,0:T(8,128)(2,1)} %param.28) | copy-start | bytes 9437188
  (2 other events, 2.2 us)
Sparse Core Ops, SparseCore 0:
  8.9 37.1 all-gather.3
  51.1 49.8 all-gather.7
  103.1 47.6 all-gather.5
  249.7 43.0 reduce-scatter.1
where the time goes:
time: 300 us; the launch traced here: 299 us
  waiting for transfers between devices  144 us (48%)
  matrix products  84.8 us (28%)
  other arithmetic  34.7 us (12%)
  local copies, waits for them, and re-layouts  14.3 us (5%)
  between operations  14.1 us (5%)
  starting transfers between devices  6.77 us (2%)
    all_gather x1, waiting for transfers between devices, diff_part(): lax.all_gather(diff_k, 'sp', axis=0, tiled=True)  49.8 us
    reduce_scatter x1, waiting for transfers between devices, body(): lax.psum_scatter((partial_value + jnp.dot(diff_rows, diff_out, preferred_...  43.2 us
    all_gather x1, waiting for transfers between devices, body(): segment = lax.all_gather(inputs, 'tp', axis=1, tiled=True)  38.8 us
    dot_general x4, matrix products, one_key_block(): jnp.einsum('hmqk,khd->hmqd', exponent.astype(jnp.bfloat16), value_slab, p...  37.3 us
    dot_general x6, matrix products, body(): jnp.dot(segment, weight, preferred_element_type=jnp.float32)  19.8 us
    reduce_sum x4, other arithmetic, one_key_block(): new_total = block_sum * rescale + jnp.sum(exponent, axis=-1)  19.5 us
    all_gather x1, waiting for transfers between devices, diff_part(): lax.all_gather(diff_v, 'sp', axis=0, tiled=True)  11.3 us
    dot_general x4, matrix products, one_key_block(): jnp.einsum('qhmd,khmd->hmqk', query_slab, key_slab, preferred_element_typ...  11 us
  transfers between devices with their start and end apart: 6, of which 4 were waited for; matrix products, arithmetic and copies ran while one was open for 10% of the time, Pallas kernels for 0%

commit v1 on v0

--- a/solution.py
+++ b/solution.py
@@ -166,7 +166,14 @@
     row_count = inputs.shape[0]
     live_count = length[0]
     weights = (win_query, win_key, win_value, diff_query, diff_key, diff_value)
-    segment = lax.all_gather(inputs, "tp", axis=1, tiled=True)
+    size = lax.axis_size("tp")
+    right = [(i_2, (i_2 + 1) % size) for i_2 in range(size)]
+    blocks = [inputs]
+    for hop in range(1, size):
+        blocks = [lax.ppermute(blocks[0], "tp", right), *blocks]
+    result_2 = jnp.concatenate(blocks, axis=1)
+    places = (lax.axis_index("tp") + 1) * blocks[-1].shape[1]
+    segment = jnp.roll(result_2, places, axis=1)
     summed = tuple(
         (jnp.dot(segment, weight, preferred_element_type=jnp.float32) for weight in weights)
     )

time: 300 us -> 316 us (1.053)
  local copies, waits for them, and re-layouts: 14.3 us -> 26.4 us
  matrix products: 84.8 us -> 88.6 us
    ppermute x0 -> x3, waiting for transfers between devices: none -> 43.4 us  [body(): blocks = [lax.ppermute(blocks[0], 'tp', right), *blocks]]
    all_gather x1, waiting for transfers between devices: 49.8 us -> 6.7 us  [diff_part(): lax.all_gather(diff_k, 'sp', axis=0, tiled=True)]
    all_gather x1 -> x0, waiting for transfers between devices: 38.8 us -> none  [body(): segment = lax.all_gather(inputs, 'tp', axis=1, tiled=True)]
    all_gather x1, waiting for transfers between devices: 11.3 us -> 49.8 us  [diff_part(): lax.all_gather(diff_v, 'sp', axis=0, tiled=True)]
    unnamed x32 -> x39, local copies, waits for them, and re-layouts: 0.7 us -> 12.7 us
  transfers between devices with their start and end apart: 6 -> 8, of which waited for: 4 -> 6; matrix products, arithmetic and copies ran while one was open for 10% -> 12% of each run, Pallas kernels for 0% -> 0%
where the time goes in v1:
time: 316 us; the launch traced here: 315 us
  waiting for transfers between devices  143 us (45%)
  matrix products  88.6 us (28%)
  other arithmetic  34.7 us (11%)
  local copies, waits for them, and re-layouts  26.4 us (8%)
  between operations  14 us (4%)
  starting transfers between devices  7.58 us (2%)
    all_gather x1, waiting for transfers between devices, diff_part(): lax.all_gather(diff_v, 'sp', axis=0, tiled=True)  49.8 us
    ppermute x3, waiting for transfers between devices, body(): blocks = [lax.ppermute(blocks[0], 'tp', right), *blocks]  43.4 us
    reduce_scatter x1, waiting for transfers between devices, body(): lax.psum_scatter((partial_value + jnp.dot(diff_rows, diff_out, preferred_...  43.3 us
    dot_general x4, matrix products, one_key_block(): jnp.einsum('hmqk,khd->hmqd', exponent.astype(jnp.bfloat16), value_slab, p...  37.2 us
    dot_general x6, matrix products, body(): jnp.dot(segment, weight, preferred_element_type=jnp.float32)  23 us
    reduce_sum x4, other arithmetic, one_key_block(): new_total = block_sum * rescale + jnp.sum(exponent, axis=-1)  19.5 us
    unnamed x39, local copies, waits for them, and re-layouts  12.7 us
    dot_general x4, matrix products, one_key_block(): jnp.einsum('qhmd,khmd->hmqk', query_slab, key_slab, preferred_element_typ...  11 us
  transfers between devices with their start and end apart: 8, of which 6 were waited for; matrix products, arithmetic and copies ran while one was open for 12% of the time, Pallas kernels for 0%

profile of v1, /device:TPU:0, one launch (start us, length us, event | category | flops | bytes accessed | tf_op | source)
XLA Modules:
  0.0 315.2 jit_solution(3632788154810961132)
XLA Ops:
  7.0 14.6 %collective-permute-done = bf16[512,1024]{1,0:T(8,128)(2,1)S(1)} collective-permute-done((bf16[512,1024]{1,0:T(8,128)(2,1)}, bf16[512,1024]{1,0:T(8,128)(2,1)S(1)}, u32[]{:S(2)}, u32[]{:S(2)}) %collective-permute-start) | collective-permute-done | bytes 1048608 | tf_op jit(solution)/shard_map/ppermute | solution.py:173
  22.7 14.3 %collective-permute-done.1 = bf16[512,1024]{1,0:T(8,128)(2,1)} collective-permute-done((bf16[512,1024]{1,0:T(8,128)(2,1)S(1)}, bf16[512,1024]{1,0:T(8,128)(2,1)}, u32[]{:S(2)}, u32[]{:S(2)}) %collective-permute-start.1) | collective-permute-done | bytes 1048608 | tf_op jit(solution)/shard_map/ppermute | solution.py:173
  37.0 14.5 %collective-permute-done.2 = bf16[512,1024]{1,0:T(8,128)(2,1)} collective-permute-done((bf16[512,1024]{1,0:T(8,128)(2,1)}, bf16[512,1024]{1,0:T(8,128)(2,1)}, u32[]{:S(2)}, u32[]{:S(2)}) %collective-permute-start.2) | collective-permute-done | bytes 1048608 | tf_op jit(solution)/shard_map/ppermute | solution.py:173
  66.3 4.3 %fusion.61 = bf16[512,128]{0,1:T(8,128)(2,1)S(1)} fusion(bf16[4096,128]{1,0:T(8,128)(2,1)} %param.21, bf16[512,8192]{1,0:T(8,128)(2,1)} %copy-done.10, s32[]{:T(128)S(6)} %select_n.62), kind=kOutput, calls=%fused_computation.50 | convolution fusion | flops 536936448 | bytes 5373956 | tf_op jit(solution)/shard_map/dot_general | solution.py:178
  70.7 4.0 %fusion.58 = bf16[512,128]{0,1:T(8,128)(2,1)S(1)} fusion(bf16[4096,128]{1,0:T(8,128)(2,1)} %param.20, bf16[512,8192]{1,0:T(8,128)(2,1)} %copy-done.10, s32[]{:T(128)S(6)} %select_n.62), kind=kOutput, calls=%fused_computation.49 | convolution fusion | flops 536936448 | bytes 5373956 | tf_op jit(solution)/shard_map/dot_general | solution.py:178
  77.9 5.5 %collective-permute-start.3 = (bf16[128,256]{0,1:T(8,128)(2,1)}, bf16[128,256]{0,1:T(8,128)(2,1)}, u32[]{:S(2)}, u32[]{:S(2)}) collective-permute-start(bf16[128,256]{0,1:T(8,128)(2,1)} %bitcast.8), channel_id=1, source_target_pairs={{0,4},{4,8},{8,12},{12,16},{16,20},{20,24},{24,28},{1,5},{5,9},{9,... | collective-permute-start | bytes 196616 | tf_op jit(solution)/shard_map/ppermute | solution.py:19
  85.4 5.8 %fusion.46 = bf16[512,384]{0,1:T(8,128)(2,1)} fusion(bf16[4096,384]{1,0:T(8,128)(2,1)} %param.19, bf16[512,8192]{1,0:T(8,128)(2,1)} %copy-done.10, s32[]{:T(128)S(6)} %select_n.62), kind=kOutput, calls=%fused_computation.45 | convolution fusion | flops 1610809344 | bytes 7733252 | tf_op jit(solution)/shard_map/dot_general | solution.py:178
  91.4 4.9 %fusion.49 = bf16[512,256]{1,0:T(8,128)(2,1)} fusion(bf16[4096,256]{1,0:T(8,128)(2,1)} %param.23, bf16[512,8192]{1,0:T(8,128)(2,1)} %copy-done.10, s32[]{:T(128)S(6)} %select_n.62), kind=kOutput, calls=%fused_computation.46 | convolution fusion | flops 1073872896 | bytes 6553604 | tf_op jit(solution)/shard_map/dot_general | solution.py:178
  104.2 5.6 %fusion.88 = f32[512,4096]{1,0:T(8,128)} fusion(bf16[512,384]{0,1:T(8,128)(2,1)S(1)} %bitcast.117, bf16[384,4096]{1,0:T(8,128)(2,1)S(1)} %copy-done), kind=kOutput, calls=%fused_computation.94 | convolution fusion | flops 1610612736 | bytes 11927552 | tf_op jit(solution)/shard_map/dot_general | solution.py:184
  109.8 6.7 %all-gather.3.cloned.1.call-done = bf16[4096,256]{1,0:T(8,128)(2,1)} async-done(((bf16[512,256]{1,0:T(8,128)(2,1)}), bf16[4096,256]{1,0:T(8,128)(2,1)}) %all-gather.3.cloned.1.call-update) | async-done | bytes 2097168 | tf_op jit(solution)/shard_map/all_gather | solution.py:125
  116.5 49.8 %all-gather.5.cloned.1.call-done = bf16[4096,256]{1,0:T(8,128)(2,1)} async-done(((bf16[512,256]{1,0:T(8,128)(2,1)}), bf16[4096,256]{1,0:T(8,128)(2,1)}) %all-gather.5.cloned.1.call-update) | async-done | bytes 2097168 | tf_op jit(solution)/shard_map/all_gather | solution.py:126
  166.3 89.2 %conditional.1 = (f32[4,2,512]{2,1,0:T(2,128)}, f32[4,2,512,64]{2,3,1,0:T(8,128)}) conditional(s32[]{:T(128)} %convert_element_type.55, () %tuple.29, (s32[512]{0:T(512)S(1)}, bf16[512,256]{1,0:T(8,128)(2,1)S(1)}, bf16[4096,256]{1,0:T(8,128)(2,1)}, bf16[4096,256]{1,0:T(8,128)(2,1)}, s32[]{:T(128)}, /*index=5*/s32[]{:T(128)}) %tuple.72), branch_computations={%region_3.4_spmd, %region_4.9_spmd.clone} | conditional | flops 859970048 | bytes 132364824 | solution.py:127
  167.7 4.1 %copy.34 = bf16[4096,256]{0,1:T(8,128)(2,1)} copy(bf16[4096,256]{1,0:T(8,128)(2,1)} %get-tuple-element.232) | data formatting | bytes 4194304 | tf_op jit(solution)/shard_map
  176.5 79.0 %while.33 = (s32[]{:T(128)}, f32[4,2,512]{2,1,0:T(2,128)S(1)}, f32[4,2,512]{2,1,0:T(2,128)}, f32[4,2,512,64]{2,3,1,0:T(8,128)}, s32[]{:T(128)}, /*index=5*/s32[]...) while((s32[]{:T(128)}, f32[4,2,512]{2,1,0:T(2,128)S(1)}, ...), condition=%wide.region_8.8_spmd, body=%wide.region_5.7_spmd.sunk | while | flops 859969536 | bytes 122368224 | solution.py:109
  179.9 4.9 %fusion.113 = f32[4,2,128]{2,1,0:T(2,128)S(1)} fusion(f32[4,2,128,4096]{3,2,1,0:T(8,128)S(1)} %get-tuple-element.339, f32[4,2,128]{2,1,0:T(2,128)S(1)} %get-tuple-element.340, pred[4096]{0:T(1024)(128)(4,1)S(1)} %iota_compare_fusion.2), kind=kLoop, calls=%fused_computation.4.clone.1 | loop fusion | flops 20970496 | bytes 16789504 | tf_op jit(solution)/shard_map/cond/branch_1_fun/while/body/while/body/eval_jaxpr/reduce_sum | solution.py:93
  186.9 9.3 %fusion.114 = f32[4,2,512,64]{2,3,1,0:T(8,128)} fusion(f32[4,2,512,64]{2,3,1,0:T(8,128)} %get-tuple-element.359, s32[]{:T(128)S(6)} %select_n.141, bf16[4096,4,64]{0,2,1:T(8,128)(2,1)} %get-tuple-element.377, f32[4,2,128,4096]{3,2,1,0:T(8,128)} %copy-done.2, f32[4,2,128]{2,1,0:T(2,128)S(1)} %get-tuple-element.340, ...), kind=kOutput, calls=%fused_computation.9.clone.1 | convolution fusion | flops 557973504 | bytes 19410948 | tf_op jit(solution)/shard_map/cond/branch_1_fun/while/body/while/body/eval_jaxpr/hmqk,khd->hmqd/dot_general | solution.py:94
  199.7 4.9 %fusion.113 = f32[4,2,128]{2,1,0:T(2,128)S(1)} fusion(f32[4,2,128,4096]{3,2,1,0:T(8,128)S(1)} %get-tuple-element.339, f32[4,2,128]{2,1,0:T(2,128)S(1)} %get-tuple-element.340, pred[4096]{0:T(1024)(128)(4,1)S(1)} %iota_compare_fusion.2), kind=kLoop, calls=%fused_computation.4.clone.1 | loop fusion | flops 20970496 | bytes 16789504 | tf_op jit(solution)/shard_map/cond/branch_1_fun/while/body/while/body/eval_jaxpr/reduce_sum | solution.py:93
  206.7 9.3 %fusion.114 = f32[4,2,512,64]{2,3,1,0:T(8,128)} fusion(f32[4,2,512,64]{2,3,1,0:T(8,128)} %get-tuple-element.359, s32[]{:T(128)S(6)} %select_n.141, bf16[4096,4,64]{0,2,1:T(8,128)(2,1)} %get-tuple-element.377, f32[4,2,128,4096]{3,2,1,0:T(8,128)} %copy-done.2, f32[4,2,128]{2,1,0:T(2,128)S(1)} %get-tuple-element.340, ...), kind=kOutput, calls=%fused_computation.9.clone.1 | convolution fusion | flops 557973504 | bytes 19410948 | tf_op jit(solution)/shard_map/cond/branch_1_fun/while/body/while/body/eval_jaxpr/hmqk,khd->hmqd/dot_general | solution.py:94
  219.4 4.9 %fusion.113 = f32[4,2,128]{2,1,0:T(2,128)S(1)} fusion(f32[4,2,128,4096]{3,2,1,0:T(8,128)S(1)} %get-tuple-element.339, f32[4,2,128]{2,1,0:T(2,128)S(1)} %get-tuple-element.340, pred[4096]{0:T(1024)(128)(4,1)S(1)} %iota_compare_fusion.2), kind=kLoop, calls=%fused_computation.4.clone.1 | loop fusion | flops 20970496 | bytes 16789504 | tf_op jit(solution)/shard_map/cond/branch_1_fun/while/body/while/body/eval_jaxpr/reduce_sum | solution.py:93
  226.4 9.3 %fusion.114 = f32[4,2,512,64]{2,3,1,0:T(8,128)} fusion(f32[4,2,512,64]{2,3,1,0:T(8,128)} %get-tuple-element.359, s32[]{:T(128)S(6)} %select_n.141, bf16[4096,4,64]{0,2,1:T(8,128)(2,1)} %get-tuple-element.377, f32[4,2,128,4096]{3,2,1,0:T(8,128)} %copy-done.2, f32[4,2,128]{2,1,0:T(2,128)S(1)} %get-tuple-element.340, ...), kind=kOutput, calls=%fused_computation.9.clone.1 | convolution fusion | flops 557973504 | bytes 19410948 | tf_op jit(solution)/shard_map/cond/branch_1_fun/while/body/while/body/eval_jaxpr/hmqk,khd->hmqd/dot_general | solution.py:94
  239.2 4.9 %fusion.113 = f32[4,2,128]{2,1,0:T(2,128)S(1)} fusion(f32[4,2,128,4096]{3,2,1,0:T(8,128)S(1)} %get-tuple-element.339, f32[4,2,128]{2,1,0:T(2,128)S(1)} %get-tuple-element.340, pred[4096]{0:T(1024)(128)(4,1)S(1)} %iota_compare_fusion.2), kind=kLoop, calls=%fused_computation.4.clone.1 | loop fusion | flops 20970496 | bytes 16789504 | tf_op jit(solution)/shard_map/cond/branch_1_fun/while/body/while/body/eval_jaxpr/reduce_sum | solution.py:93
  246.2 9.3 %fusion.114 = f32[4,2,512,64]{2,3,1,0:T(8,128)} fusion(f32[4,2,512,64]{2,3,1,0:T(8,128)} %get-tuple-element.359, s32[]{:T(128)S(6)} %select_n.141, bf16[4096,4,64]{0,2,1:T(8,128)(2,1)} %get-tuple-element.377, f32[4,2,128,4096]{3,2,1,0:T(8,128)} %copy-done.2, f32[4,2,128]{2,1,0:T(2,128)S(1)} %get-tuple-element.340, ...), kind=kOutput, calls=%fused_computation.9.clone.1 | convolution fusion | flops 557973504 | bytes 19410948 | tf_op jit(solution)/shard_map/cond/branch_1_fun/while/body/while/body/eval_jaxpr/hmqk,khd->hmqd/dot_general | solution.py:94
  258.0 7.4 %add_convert_fusion = bf16[512,4096]{1,0:T(8,128)(2,1)} fusion(f32[512,4096]{1,0:T(8,128)} %fusion.88, bf16[512,256]{0,1:T(8,128)(2,1)S(1)} %bitcast.112, bf16[256,4096]{1,0:T(8,128)(2,1)} %param.29), kind=kOutput, calls=%fused_computation.23 | convolution fusion | flops 1077936128 | bytes 14942208 | tf_op jit(solution)/shard_map/dot_general | solution.py:186
  265.4 43.3 %reduce-scatter.2.cloned.1.call-done = bf16[128,4096]{1,0:T(8,128)(2,1)} async-done(((bf16[512,4096]{1,0:T(8,128)(2,1)}), bf16[128,4096]{1,0:T(8,128)(2,1)}) %reduce-scatter.2.cloned.1.call-update) | async-done | bytes 1048592 | tf_op jit(solution)/shard_map/reduce_scatter | solution.py:185
  (112 shorter events, 58.8 us)
Async XLA Ops:
  6.5 97.6 %copy-start = (bf16[384,4096]{1,0:T(8,128)(2,1)S(1)}, bf16[384,4096]{1,0:T(8,128)(2,1)}, u32[]{:S(2)}) copy-start(bf16[384,4096]{1,0:T(8,128)(2,1)} %param.28) | copy-start | bytes 9437188
  6.5 109.9 %all-gather.3.cloned.1.call-start = ((), (), s32[]{:S(2)}) async-start(), calls=%async_computation.1 | async-start | bytes 2359296 | tf_op jit(solution)/shard_map/all_gather | solution.py:125
  6.5 15.1 %collective-permute-start = (bf16[512,1024]{1,0:T(8,128)(2,1)}, bf16[512,1024]{1,0:T(8,128)(2,1)S(1)}, u32[]{:S(2)}, u32[]{:S(2)}) collective-permute-start(bf16[512,1024]{1,0:T(8,128)(2,1)} %param.17), channel_id=1, source_target_pairs={{0,1},{1,2},{2,3},{3,0},{4,5},{5,6},{6,7},{7,4},{8,9},{9,10},{10,1... | collective-permute-start | bytes 3145736 | tf_op jit(solution)/shard_map/ppermute | solution.py:173
  22.6 14.3 %collective-permute-start.1 = (bf16[512,1024]{1,0:T(8,128)(2,1)S(1)}, bf16[512,1024]{1,0:T(8,128)(2,1)}, u32[]{:S(2)}, u32[]{:S(2)}) collective-permute-start(bf16[512,1024]{1,0:T(8,128)(2,1)S(1)} %collective-permute-done), channel_id=1, source_target_pairs={{0,1},{1,2},{2,3},{3,0},{4,5},{5,6},{6,7},{7,4},{8,9},{9,10},{10,1... | collective-permute-start | bytes 3145736 | tf_op jit(solution)/shard_map/ppermute | solution.py:173
  36.9 14.5 %collective-permute-start.2 = (bf16[512,1024]{1,0:T(8,128)(2,1)}, bf16[512,1024]{1,0:T(8,128)(2,1)}, u32[]{:S(2)}, u32[]{:S(2)}) collective-permute-start(bf16[512,1024]{1,0:T(8,128)(2,1)} %collective-permute-done.1), channel_id=1, source_target_pairs={{0,1},{1,2},{2,3},{3,0},{4,5},{5,6},{6,7},{7,4},{8,9},{9,10},{10,1... | collective-permute-start | bytes 3145736 | tf_op jit(solution)/shard_map/ppermute | solution.py:173
  36.9 22.3 %copy-start.5 = (bf16[512,1024]{1,0:T(8,128)(2,1)S(1)}, bf16[512,1024]{1,0:T(8,128)(2,1)}, u32[]{:S(2)}) copy-start(bf16[512,1024]{1,0:T(8,128)(2,1)} %copy-done.4) | copy-start | bytes 3145732
  36.9 22.4 %copy-start.3 = (bf16[512,1024]{1,0:T(8,128)(2,1)S(1)}, bf16[512,1024]{1,0:T(8,128)(2,1)}, u32[]{:S(2)}) copy-start(bf16[512,1024]{1,0:T(8,128)(2,1)} %param.17) | copy-start | bytes 3145732
  36.9 25.7 %copy-start.14 = (bf16[4096,256]{1,0:T(8,128)(2,1)S(1)}, bf16[4096,256]{1,0:T(8,128)(2,1)}, u32[]{:S(2)}) copy-start(bf16[4096,256]{1,0:T(8,128)(2,1)} %param.24) | copy-start | bytes 6291460
  56.7 8.7 %copy-start.16 = (f32[6]{0:T(128)S(1)}, f32[6]{0:T(128)}, u32[]{:S(2)}) copy-start(f32[6]{0:T(128)} %param.22) | copy-start | bytes 76
  64.7 101.6 %all-gather.5.cloned.1.call-start = ((), (), s32[]{:S(2)}) async-start(), calls=%async_computation.2 | async-start | bytes 2359296 | tf_op jit(solution)/shard_map/all_gather | solution.py:126
  65.5 17.9 %copy-start.11 = (bf16[512,8192]{1,0:T(8,128)(2,1)S(1)}, bf16[512,8192]{1,0:T(8,128)(2,1)}, u32[]{:S(2)}) copy-start(bf16[512,8192]{1,0:T(8,128)(2,1)} %copy-done.10) | copy-start | bytes 25165828
  65.5 17.9 %copy-start.15 = (bf16[4096,256]{1,0:T(8,128)(2,1)S(1)}, bf16[4096,256]{1,0:T(8,128)(2,1)}, u32[]{:S(2)}) copy-start(bf16[4096,256]{1,0:T(8,128)(2,1)} %param.25) | copy-start | bytes 6291460
  76.6 19.7 %collective-permute-start.4 = (bf16[128,256]{0,1:T(8,128)(2,1)}, bf16[128,256]{0,1:T(8,128)(2,1)}, u32[]{:S(2)}, u32[]{:S(2)}) collective-permute-start(bf16[128,256]{0,1:T(8,128)(2,1)} %bitcast.10), channel_id=1, source_target_pairs={{4,0},{8,4},{12,8},{16,12},{20,16},{24,20},{28,24},{5,1},{9,5},{13... | collective-permute-start | bytes 196616 | tf_op jit(solution)/shard_map/ppermute | solution.py:22
  77.9 18.4 %collective-permute-start.3 = (bf16[128,256]{0,1:T(8,128)(2,1)}, bf16[128,256]{0,1:T(8,128)(2,1)}, u32[]{:S(2)}, u32[]{:S(2)}) collective-permute-start(bf16[128,256]{0,1:T(8,128)(2,1)} %bitcast.8), channel_id=1, source_target_pairs={{0,4},{4,8},{8,12},{12,16},{16,20},{20,24},{24,28},{1,5},{5,9},{9,... | collective-permute-start | bytes 196616 | tf_op jit(solution)/shard_map/ppermute | solution.py:19
  91.2 217.5 %reduce-scatter.2.cloned.1.call-start = ((), (), s32[]{:S(2)}) async-start(), calls=%async_computation.3 | async-start | bytes 5242880 | tf_op jit(solution)/shard_map/reduce_scatter | solution.py:185
  91.4 5.9 %copy-start.8 = (bf16[512,384]{0,1:T(8,128)(2,1)S(1)}, bf16[512,384]{0,1:T(8,128)(2,1)}, u32[]{:S(2)}) copy-start(bf16[512,384]{0,1:T(8,128)(2,1)} %fusion.46) | copy-start | bytes 1179652
  104.2 62.1 %copy-start.9 = (bf16[512,256]{1,0:T(8,128)(2,1)S(1)}, bf16[512,256]{1,0:T(8,128)(2,1)}, u32[]{:S(2)}) copy-start(bf16[512,256]{1,0:T(8,128)(2,1)} %fusion.49) | copy-start | bytes 786436
  166.3 91.4 %copy-start.12 = (f32[4]{0:T(128)S(1)}, f32[4]{0:T(128)}, u32[]{:S(2)}) copy-start(f32[4]{0:T(128)} %param.26) | copy-start | bytes 52
  166.3 91.6 %copy-start.13 = (f32[64]{0:T(128)S(1)}, f32[64]{0:T(128)}, u32[]{:S(2)}) copy-start(f32[64]{0:T(128)} %param.27) | copy-start | bytes 772
  179.9 5.7 %copy-start.2 = (f32[4,2,128,4096]{3,2,1,0:T(8,128)}, f32[4,2,128,4096]{3,2,1,0:T(8,128)S(1)}, u32[]{:S(2)}) copy-start(f32[4,2,128,4096]{3,2,1,0:T(8,128)S(1)} %get-tuple-element.339) | copy-start | bytes 50331652 | tf_op jit(solution)/shard_map/cond/branch_1_fun/while
  199.6 5.7 %copy-start.2 = (f32[4,2,128,4096]{3,2,1,0:T(8,128)}, f32[4,2,128,4096]{3,2,1,0:T(8,128)S(1)}, u32[]{:S(2)}) copy-start(f32[4,2,128,4096]{3,2,1,0:T(8,128)S(1)} %get-tuple-element.339) | copy-start | bytes 50331652 | tf_op jit(solution)/shard_map/cond/branch_1_fun/while
  219.4 5.7 %copy-start.2 = (f32[4,2,128,4096]{3,2,1,0:T(8,128)}, f32[4,2,128,4096]{3,2,1,0:T(8,128)S(1)}, u32[]{:S(2)}) copy-start(f32[4,2,128,4096]{3,2,1,0:T(8,128)S(1)} %get-tuple-element.339) | copy-start | bytes 50331652 | tf_op jit(solution)/shard_map/cond/branch_1_fun/while
  239.2 5.7 %copy-start.2 = (f32[4,2,128,4096]{3,2,1,0:T(8,128)}, f32[4,2,128,4096]{3,2,1,0:T(8,128)S(1)}, u32[]{:S(2)}) copy-start(f32[4,2,128,4096]{3,2,1,0:T(8,128)S(1)} %get-tuple-element.339) | copy-start | bytes 50331652 | tf_op jit(solution)/shard_map/cond/branch_1_fun/while
  258.0 50.7 %copy-start.1 = (bf16[384,4096]{1,0:T(8,128)(2,1)S(1)}, bf16[384,4096]{1,0:T(8,128)(2,1)}, u32[]{:S(2)}) copy-start(bf16[384,4096]{1,0:T(8,128)(2,1)} %param.28) | copy-start | bytes 9437188
  (4 other events, 8.9 us)
Sparse Core Ops, SparseCore 0:
  64.8 51.6 all-gather.2
  118.6 47.6 all-gather.4
  265.6 43.1 reduce-scatter.1
